TPU v7x, 32 devices: a whole 2x2x4 slice. The times are simulated.
32 devices in a mesh: sp: 16 (over z, y, x), tp: 2 (over core).
Axes of the slice: x: 2, y: 2, z: 4, core: 2. Of those that a mesh axis runs over, the one named last changes fastest.
Arguments:
- queries: bfloat16 [4096, 1024], P('sp', 'tp'), may hold values from -6 to 6
- key_vectors: bfloat16 [4096, 1024], P('sp', 'tp'), may hold values from -6 to 6
- value_vectors: bfloat16 [4096, 1024], P('sp', 'tp'), may hold values from -6 to 6
- gate_inputs: bfloat16 [4096, 1024], P('sp', 'tp'), may hold values from -6 to 6
- log_decay: float32 [4096, 16], P('sp', 'tp'), may hold values from -1 to 0
- head_gain: float32 [1024], P('tp'), may hold values from 0.1 to 1.9
- out_weight: bfloat16 [1024, 2048], P('tp'), may hold values from -0.1875 to 0.1875
- residual: bfloat16 [4096, 2048], P(('sp', 'tp')), may hold values from -6 to 6
- norm_gain: float32 [2048], replicated, may hold values from 0.1 to 1.9
- expert_ids: int32 [4096, 2], P(('sp', 'tp')), may hold values from 0 to 15, all different within a row; in each aligned block of 128 rows (0 to 127, 128 to 255, ...) at most 32 rows name the same one
- expert_weights: float32 [4096, 2], P(('sp', 'tp')), may hold values from 0.2 to 1
- gate_experts: bfloat16 [16, 2048, 3584], P('sp', None, 'tp'), may hold values from -0.125 to 0.125
- up_experts: bfloat16 [16, 2048, 3584], P('sp', None, 'tp'), may hold values from -0.125 to 0.125
- down_experts: bfloat16 [16, 3584, 2048], P('sp', 'tp'), may hold values from -0.09375 to 0.09375
Outputs:
- layer_out: bfloat16 [4096, 2048], P(('sp', 'tp'))
Inputs may be any that keep to these rules, and one draw needn't show every extreme that they name: `expert_ids`: the 2 experts of a token differ. No expert is named more than 32 times in the rows of one device, and in some device some expert is named exactly 32 times.
All inputs are finite; a program needn't handle non-finite values.
Results may differ from a plain program's by a relative error of at most 0.014.
Values may be sent and summed in bfloat16 or wider, within the bound.
A program may use at most 128 MiB of HBM per device.

v0:
```python
import jax
import jax.numpy as jnp
from jax import lax
from jax.sharding import PartitionSpec as P

BLOCK = 128


def prefix(value, axis, join, neutral):
    place = lax.axis_index(axis)
    gathered = jax.tree.map(
        lambda a, kind: lax.all_gather(a.astype(kind), axis), value, (jnp.bfloat16, jnp.bfloat16)
    )
    state = jax.tree.map(lambda a, e: jnp.zeros_like(a) + jnp.asarray(e, a.dtype), value, neutral)

    def one(hop, state):
        return join(
            state,
            jax.tree.map(
                lambda a, own: lax.dynamic_index_in_dim(a, hop, 0, False).astype(own.dtype),
                gathered,
                value,
            ),
        )

    return lax.fori_loop(0, place, one, state)


def rotate(block, places):
    half_size = block.shape[-1] // 2
    frequency = 10000.0 ** (-jnp.arange(half_size, dtype=jnp.float32) / half_size)
    angles = places.astype(jnp.float32)[:, None, None] * frequency
    first_half = block[..., :half_size]
    second = block[..., half_size:]
    return jnp.concatenate(
        [
            first_half * jnp.cos(angles) - second * jnp.sin(angles),
            second * jnp.cos(angles) + first_half * jnp.sin(angles),
        ],
        axis=-1,
    )


def to_blocks(source, blocks):
    shaped = source.reshape((blocks, source.shape[0] // blocks) + source.shape[1:])
    return jnp.swapaxes(shaped, 1, 2)


def from_blocks(source):
    shaped = jnp.swapaxes(source, 1, 2)
    return shaped.reshape((shaped.shape[0] * shaped.shape[1],) + shaped.shape[2:])


def block_step(carried_state, inputs):
    query_rows, key_rows, value_rows, decay_rows = inputs
    cumulative = jnp.cumsum(decay_rows, axis=1)
    log_gaps = cumulative[:, :, None] - cumulative[:, None, :]
    offsets = jnp.arange(decay_rows.shape[1])
    causal = offsets[:, None] >= offsets[None, :]
    decay_weight = jnp.where(causal, jnp.exp(jnp.where(causal, log_gaps, 0.0)), 0.0)
    scores = (
        jnp.einsum("htd,hsd->hts", query_rows, key_rows, precision=lax.Precision.HIGHEST)
        * decay_weight
    )
    within = jnp.einsum("hts,hse->hte", scores, value_rows, precision=lax.Precision.HIGHEST)
    carried = jnp.einsum(
        "htd,hde->hte",
        query_rows * jnp.exp(cumulative)[:, :, None],
        carried_state,
        precision=lax.Precision.HIGHEST,
    )
    last_log = cumulative[:, -1:]
    fresh_state = jnp.einsum(
        "hsd,hse->hde",
        key_rows * jnp.exp(last_log - cumulative)[:, :, None],
        value_rows,
        precision=lax.Precision.HIGHEST,
    )
    return (jnp.exp(last_log)[:, :, None] * carried_state + fresh_state, within + carried)


def link_states(earlier, later):
    return (earlier[0] + later[0], jnp.exp(later[0])[:, None, None] * earlier[1] + later[1])


def expert_hidden(batch, gate_matrix, up_matrix):
    gate_value = jnp.dot(batch, gate_matrix, preferred_element_type=jnp.float32)
    up_value = jnp.dot(batch, up_matrix, preferred_element_type=jnp.float32)
    return (jax.nn.silu(gate_value) * up_value).astype(jnp.bfloat16)


def shards(
    queries,
    key_vectors,
    value_vectors,
    gate_inputs,
    log_decay,
    head_gain,
    out_weight,
    residual,
    norm_gain,
    expert_ids,
    expert_weights,
    gate_experts,
    up_experts,
    down_experts,
):
    tok_dev, channels = queries.shape
    head_count = log_decay.shape[1]
    head_size = channels // head_count
    blocks = tok_dev // BLOCK
    places = lax.axis_index("sp") * tok_dev + jnp.arange(tok_dev, dtype=jnp.int32)
    turned_queries = rotate(
        queries.astype(jnp.float32).reshape(tok_dev, head_count, head_size), places
    )
    turned_keys = rotate(
        key_vectors.astype(jnp.float32).reshape(tok_dev, head_count, head_size), places
    ) * head_size ** (-0.5)
    value_float = value_vectors.astype(jnp.float32).reshape(tok_dev, head_count, head_size)
    inputs = (
        to_blocks(turned_queries, blocks),
        to_blocks(turned_keys, blocks),
        to_blocks(value_float, blocks),
        to_blocks(log_decay, blocks),
    )
    zero_state = jnp.zeros((head_count, head_size, head_size), jnp.float32)
    running = jnp.cumsum(log_decay, axis=0)
    device_total = running[-1]
    identity = (jnp.zeros_like(device_total), zero_state)
    end_weight = jnp.exp(device_total[None, :] - running)
    local_end = jnp.einsum(
        "thd,the->hde",
        turned_keys * end_weight[:, :, None],
        value_float,
        precision=lax.Precision.HIGHEST,
    )
    _, incoming = prefix((device_total, local_end), "sp", link_states, identity)
    _, pieces = lax.scan(block_step, incoming, inputs)
    retained = from_blocks(pieces)
    squares = jnp.mean(retained * retained, axis=-1, keepdims=True)
    normed = retained * lax.rsqrt(squares + 1e-06) * head_gain.reshape(head_count, head_size)
    normed = (
        normed.reshape(tok_dev, channels) * jax.nn.silu(gate_inputs.astype(jnp.float32))
    ).astype(jnp.bfloat16)
    projected = lax.psum_scatter(
        jnp.dot(normed, out_weight, preferred_element_type=jnp.float32).astype(jnp.bfloat16),
        "tp",
        scatter_dimension=0,
        tiled=True,
    ).astype(jnp.float32)
    mixed_rows = (residual.astype(jnp.float32) + projected).astype(jnp.bfloat16)
    mixed_float = mixed_rows.astype(jnp.float32)
    normed_rows = (
        mixed_float
        * lax.rsqrt(jnp.mean(mixed_float * mixed_float, axis=-1, keepdims=True) + 1e-06)
        * norm_gain
    ).astype(jnp.bfloat16)
    d_model = residual.shape[1]
    experts = lax.axis_size("sp")
    capacity = 2 * tok_dev // experts
    top_count = expert_ids.shape[1]
    flat_routes = expert_ids.reshape(-1)
    onehot = (flat_routes[:, None] == jnp.arange(experts, dtype=jnp.int32)[None, :]).astype(
        jnp.int32
    )
    slot_rank = jnp.sum(jnp.cumsum(onehot, axis=0) * onehot, axis=1) - 1
    source_row = jnp.arange(flat_routes.shape[0], dtype=jnp.int32) // top_count
    outgoing = (
        jnp.zeros((experts, capacity, d_model), jnp.bfloat16)
        .at[flat_routes, slot_rank]
        .set(normed_rows[source_row])
    )
    both_halves = lax.all_gather(
        lax.all_to_all(outgoing, "sp", split_axis=0, concat_axis=0, tiled=True),
        "tp",
        axis=0,
        tiled=True,
    )
    hidden = expert_hidden(both_halves.reshape(-1, d_model), gate_experts[0], up_experts[0])
    partial_value = jnp.dot(hidden, down_experts[0], preferred_element_type=jnp.float32)
    summed = lax.psum_scatter(
        partial_value.reshape(both_halves.shape).astype(jnp.bfloat16),
        "tp",
        scatter_dimension=0,
        tiled=True,
    )
    returned = lax.all_to_all(summed, "sp", split_axis=0, concat_axis=0, tiled=True)
    picked = (
        returned[flat_routes, slot_rank].astype(jnp.float32) * expert_weights.reshape(-1)[:, None]
    )
    expert_sum = jnp.sum(picked.reshape(-1, top_count, d_model), axis=1)
    return (mixed_float + expert_sum).astype(jnp.bfloat16)


def solution(mesh):
    return jax.shard_map(
        shards,
        mesh=mesh,
        in_specs=(
            P("sp", "tp"),
            P("sp", "tp"),
            P("sp", "tp"),
            P("sp", "tp"),
            P("sp", "tp"),
            P("tp"),
            P("tp", None),
            P(("sp", "tp"), None),
            P(),
            P(("sp", "tp"), None),
            P(("sp", "tp"), None),
            P("sp", None, "tp"),
            P("sp", None, "tp"),
            P("sp", "tp", None),
        ),
        out_specs=P(("sp", "tp"), None),
        check_vma=False,
    )
```

profile of v0, /device:TPU:14, one launch (start us, length us, event | category | flops | bytes accessed | tf_op | source)
XLA Modules:
  0.0 350.8 jit_solution(12498100676336521632)
XLA Ops:
  6.6 1.3 copy.61
  7.9 1.1 copy.65
  9.0 0.8 convert.7
  9.8 1.2 reduce-window.14
  11.6 1.8 copy.62
  13.4 0.2 multiply_cosine_fusion
  13.6 2.0 multiply_subtract_fusion
  15.6 2.0 convolution_convert_fusion.1
  17.6 0.8 concatenate.18
  18.4 0.8 concatenate.19
  19.6 28.1 %all-gather.1 = bf16[16,1,8]{2,1,0:T(2,128)(2,1)S(1)} all-gather(bf16[1,1,8]{2,1,0:T(2,128)(2,1)S(1)} %bitcast.168), channel_id=1, replica_groups=mesh['sp'=16,'tp'=2] {'sp'}, dimensions={0}, use_global_device_ids=true | all-gather | bytes 272 | tf_op jit(solution)/shard_map/all_gather | solution.py:12
  47.8 1.1 pad_maximum_fusion
  48.9 1.1 reshape.309
  49.9 1.1 reshape.320
  51.0 1.8 copy.70
  52.8 1.3 fusion.28
  54.1 24.1 %all-gather.7.cloned.1.call-done = bf16[128,64,64]{2,1,0:T(8,128)(2,1)} async-done(((bf16[8,64,64]{2,1,0:T(8,128)(2,1)}), bf16[128,64,64]{2,1,0:T(8,128)(2,1)}) %all-gather.7.cloned.1.call-update) | async-done | bytes 1048592 | tf_op jit(solution)/shard_map/all_gather | solution.py:12
  78.2 7.5 %while.24 = (s32[]{:T(128)}, f32[8,64,64]{2,1,0:T(8,128)S(1)}, s32[]{:T(128)}, bf16[16,8]{1,0:T(8,128)(2,1)S(1)}, bf16[16,8,64,64]{3,2,1,0:T(8,128)(2,1)}, /*index=5*/s32[]{:T(128)}, s32[]{:T(128)}, s32[]{:T(128)}) while((s32[]{:T(128)}, f32[8,64,64]{2,1,0:T(8,128)S(1)}, s32[]{:T(128)}, bf16[16,8]{1,0:T(8,128)(2,1)S(1)}, ...), condition=%wide.region_3.4_spmd, body=%wide.region_2.3_spmd.sunk | while | flops 98317 | bytes 327887 | solution.py:26
  78.3 1.0 convert_add_fusion.3
  79.3 1.0 convert_add_fusion.3
  80.4 1.0 convert_add_fusion.3
  81.5 1.0 convert_add_fusion.3
  82.5 1.0 convert_add_fusion.3
  83.6 1.0 convert_add_fusion.3
  84.7 1.0 convert_add_fusion.3
  85.7 13.4 %while.25 = (s32[]{:T(128)}, f32[8,64,64]{2,1,0:T(8,128)S(1)}, f32[2,8,128,64]{2,3,1,0:T(8,128)}, f32[2,8,128]{2,1,0:T(8,128)S(1)}, f32[2,8,128,64]{2,0,3,1:T(2,...) while((s32[]{:T(128)}, f32[8,64,64]{2,1,0:T(8,128)S(1)}, ...), condition=%wide.region_6.7_spmd, body=%wide.region_4.6_spmd.sunk | while | flops 302923776 | bytes 5448461 | solution.py:138
  85.7 1.7 constant_dynamic-slice_fusion.5
  87.5 0.3 reduce_window_sum.49
  87.8 0.3 constant_dynamic-slice_fusion.6
  88.1 1.1 convolution_multiply_fusion.2
  89.2 1.1 fusion.72
  90.5 1.3 fusion.73
  91.8 0.6 convolution_add_fusion.3
  92.4 1.7 constant_dynamic-slice_fusion.5
  94.2 0.3 reduce_window_sum.49
  94.5 0.3 constant_dynamic-slice_fusion.6
  94.8 1.1 convolution_multiply_fusion.2
  95.9 1.1 fusion.72
  97.2 1.3 fusion.73
  98.5 0.6 convolution_add_fusion.3
  99.1 1.1 multiply_reduce_fusion.1
  100.3 1.5 copy.69
  101.8 1.2 fusion.29
  102.9 1.7 convolution_convert_fusion
  105.3 0.6 reduce-window.16
  106.2 15.5 %reduce-scatter.3.cloned.1.call-done = bf16[128,2048]{1,0:T(8,128)(2,1)} async-done(((bf16[256,2048]{1,0:T(8,128)(2,1)}), bf16[128,2048]{1,0:T(8,128)(2,1)}) %reduce-scatter.3.cloned.1.call-update) | async-done | bytes 524304 | tf_op jit(solution)/shard_map/reduce_scatter | solution.py:145
  121.8 1.3 fusion.17
  123.1 1.3 fusion.19
  124.4 2.3 gather_fusion
  126.7 0.2 broadcast_in_dim.33
  127.0 33.3 %scatter_fusion = bf16[16,32,2048]{2,1,0:T(8,128)(2,1)S(1)} fusion(bf16[16,32,2048]{2,1,0:T(8,128)(2,1)S(1)} %broadcast_in_dim.33, s32[256]{0:T(256)S(1)} %bitcast.154, bf16[256,2048]{1,0:T(8,128)(2,1)} %gather_fusion), kind=kCustom, calls=%fused_computation.2 | custom fusion | bytes 3147776 | tf_op jit(solution)/shard_map/scatter | solution.py:171
  160.3 54.0 %all_to_all.10 = bf16[16,32,2048]{2,1,0:T(8,128)(2,1)} all-to-all(bf16[16,32,2048]{2,1,0:T(8,128)(2,1)S(1)} %scatter_fusion), channel_id=1, replica_groups=mesh['sp'=16,'tp'=2] {'sp'}, dimensions={0} | all-to-all | bytes 4194304 | tf_op jit(solution)/shard_map/all_to_all | solution.py:174
  214.3 0.2 reduce-scatter.5.cloned.1.call-start
  214.5 13.8 %all-gather.5.cloned.1.call-done = bf16[32,32,2048]{2,1,0:T(8,128)(2,1)} async-done(((bf16[16,32,2048]{2,1,0:T(8,128)(2,1)}), bf16[32,32,2048]{2,1,0:T(8,128)(2,1)}) %all-gather.5.cloned.1.call-update) | async-done | bytes 4194320 | tf_op jit(solution)/shard_map/all_gather | solution.py:173
  228.4 11.8 %fusion.10 = f32[1024,1792]{1,0:T(8,128)S(1)} fusion(bf16[1024,2048]{1,0:T(8,128)(2,1)} %bitcast.172, bf16[1,2048,1792]{2,1,0:T(8,128)(2,1)} %param.29), kind=kOutput, calls=%fused_computation.26 | convolution fusion | flops 7516192768 | bytes 18874368 | tf_op jit(solution)/shard_map/dot_general | solution.py:87
  240.2 11.4 %multiply_convert_fusion = bf16[1024,1792]{1,0:T(8,128)(2,1)S(1)} fusion(f32[1024,1792]{1,0:T(8,128)S(1)} %fusion.10, bf16[1024,2048]{1,0:T(8,128)(2,1)S(1)} %bitcast.173, bf16[1,2048,1792]{2,1,0:T(8,128)(2,1)} %param.30), kind=kOutput, calls=%fused_computation.28 | convolution fusion | flops 7527202816 | bytes 22544384 | tf_op jit(solution)/shard_map/dot_general | solution.py:88
  251.6 9.3 %fusion.14 = bf16[32,32,2048]{2,1,0:T(8,128)(2,1)} fusion(bf16[32,32,1792]{2,1,0:T(8,128)(2,1)S(1)} %bitcast.174, bf16[1,1792,2048]{2,1,0:T(8,128)(2,1)S(1)} %bitcast.171), kind=kOutput, calls=%fused_computation.29 | convolution fusion | flops 7518289920 | bytes 15204352 | tf_op jit(solution)/shard_map/dot_general | solution.py:180
  260.9 13.5 %reduce-scatter.5.cloned.1.call-done = bf16[16,32,2048]{2,1,0:T(8,128)(2,1)} async-done(((bf16[32,32,2048]{2,1,0:T(8,128)(2,1)}), bf16[16,32,2048]{2,1,0:T(8,128)(2,1)}) %reduce-scatter.5.cloned.1.call-update) | async-done | bytes 2097168 | tf_op jit(solution)/shard_map/reduce_scatter | solution.py:181
  274.4 7.0 %all-to-all-start.1 = ((bf16[16,32,2048]{2,1,0:T(8,128)(2,1)}), bf16[16,32,2048]{2,1,0:T(8,128)(2,1)}, u32[]{:S(2)}, u32[]{:S(2)}) async-start(bf16[16,32,2048]{2,1,0:T(8,128)(2,1)} %reduce-scatter.5.cloned.1.call-done), calls=%async_computation.3 | async-start | bytes 4194304 | tf_op jit(solution)/shard_map/all_to_all | solution.py:187
  281.5 48.3 %all-to-all-done.1 = bf16[16,32,2048]{2,1,0:T(8,128)(2,1)} async-done(((bf16[16,32,2048]{2,1,0:T(8,128)(2,1)}), bf16[16,32,2048]{2,1,0:T(8,128)(2,1)}, u32[]{:S(2)}, u32[]{:S(2)}) %all-to-all-start.1) | async-done | bytes 2097184 | tf_op jit(solution)/shard_map/all_to_all | solution.py:187
  329.8 5.2 %gather_fusion.1 = bf16[256,2048]{1,0:T(8,128)(2,1)} fusion(bf16[16,32,2048]{2,1,0:T(8,128)(2,1)} %all-to-all-done.1, s32[256]{0:T(256)S(1)} %bitcast.153), kind=kCustom, calls=%fused_computation.1 | custom fusion | bytes 2099200 | tf_op jit(solution)/shard_map/gather | solution.py:189
  335.0 3.5 reshape.319
  338.5 4.8 %multiply_reduce_fusion = f32[128,2048]{1,0:T(8,128)S(1)} fusion(f32[128,2,2048]{2,1,0:T(2,128)} %reshape.319, f32[128,2]{1,0:T(8,128)S(1)} %copy.75), kind=kLoop, calls=%fused_computation.31 | loop fusion | flops 786432 | bytes 3146752 | tf_op jit(solution)/shard_map/reduce_sum | solution.py:191
  343.3 1.0 fusion.20
  (79 shorter events, 2.8 us)
Async XLA Ops:
  6.5 96.4 %copy-start = (bf16[512,2048]{1,0:T(8,128)(2,1)S(1)}, bf16[512,2048]{1,0:T(8,128)(2,1)}, u32[]{:S(2)}) copy-start(bf16[512,2048]{1,0:T(8,128)(2,1)} %param.24) | copy-start | bytes 6291460
  6.5 12.7 %copy-start.4 = (bf16[256,512]{1,0:T(8,128)(2,1)S(1)}, bf16[256,512]{1,0:T(8,128)(2,1)}, u32[]{:S(2)}) copy-start(bf16[256,512]{1,0:T(8,128)(2,1)} %param.20) | copy-start | bytes 786436
  6.5 71.7 %all-gather.7.cloned.1.call-start = ((), (), s32[]{:S(2)}) async-start(), calls=%async_computation.7 | async-start | bytes 2228224 | tf_op jit(solution)/shard_map/all_gather | solution.py:12
  17.6 104.2 %reduce-scatter.3.cloned.1.call-start = ((), (), s32[]{:S(2)}) async-start(), calls=%async_computation.4 | async-start | bytes 1572864 | tf_op jit(solution)/shard_map/reduce_scatter | solution.py:145
  47.8 37.9 %copy-start.5 = (f32[256,8]{0,1:T(8,128)S(1)}, f32[256,8]{0,1:T(8,128)}, u32[]{:S(2)}) copy-start(f32[256,8]{0,1:T(8,128)} %param.22) | copy-start | bytes 24580
  85.7 16.1 %copy-start.7 = (f32[512]{0:T(512)S(1)}, f32[512]{0:T(512)}, u32[]{:S(2)}) copy-start(f32[512]{0:T(512)} %param.23) | copy-start | bytes 6148
  99.1 5.6 %copy-start.8 = (s32[128,2]{0,1:T(2,128)S(1)}, s32[128,2]{0,1:T(2,128)}, u32[]{:S(2)}) copy-start(s32[128,2]{0,1:T(2,128)} %param.27) | copy-start | bytes 3076
  99.1 22.7 %copy-start.2 = (bf16[128,2048]{1,0:T(8,128)(2,1)S(1)}, bf16[128,2048]{1,0:T(8,128)(2,1)}, u32[]{:S(2)}) copy-start(bf16[128,2048]{1,0:T(8,128)(2,1)} %param.25) | copy-start | bytes 1572868
  99.1 24.0 %copy-start.6 = (f32[2048]{0:T(1024)S(1)}, f32[2048]{0:T(1024)}, u32[]{:S(2)}) copy-start(f32[2048]{0:T(1024)} %param.26) | copy-start | bytes 24580
  104.7 123.7 %all-gather.5.cloned.1.call-start = ((), (), s32[]{:S(2)}) async-start(), calls=%async_computation.5 | async-start | bytes 6291456 | tf_op jit(solution)/shard_map/all_gather | solution.py:173
  214.3 60.1 %reduce-scatter.5.cloned.1.call-start = ((), (), s32[]{:S(2)}) async-start(), calls=%async_computation.6 | async-start | bytes 6291456 | tf_op jit(solution)/shard_map/reduce_scatter | solution.py:181
  228.4 11.8 %copy-start.10 = (bf16[32,32,2048]{2,1,0:T(8,128)(2,1)S(1)}, bf16[32,32,2048]{2,1,0:T(8,128)(2,1)}, u32[]{:S(2)}) copy-start(bf16[32,32,2048]{2,1,0:T(8,128)(2,1)} %all-gather.5.cloned.1.call-done) | copy-start | bytes 12582916
  228.4 23.2 %slice-start = ((s8[7340032]{0:T(1024)(128)(4,1)}), s8[4194304]{0:T(1024)(128)(4,1)S(1)}, s32[]{:S(2)}) async-start(s8[7340032]{0:T(1024)(128)(4,1)} %bitcast.170), calls=%async_computation.8 | async-start | bytes 8388608
  240.2 11.4 %slice-start.1 = ((s8[7340032]{0:T(1024)(128)(4,1)}), s8[3145728]{0:T(1024)(128)(4,1)S(1)}, s32[]{:S(2)}) async-start(s8[7340032]{0:T(1024)(128)(4,1)} %bitcast.170), calls=%async_computation.9 | async-start | bytes 6291456
  260.9 20.5 %copy-start.9 = (f32[128,2]{0,1:T(2,128)S(1)}, f32[128,2]{0,1:T(2,128)}, u32[]{:S(2)}) copy-start(f32[128,2]{0,1:T(2,128)} %param.28) | copy-start | bytes 3076
  274.4 55.4 %all-to-all-start.1 = ((bf16[16,32,2048]{2,1,0:T(8,128)(2,1)}), bf16[16,32,2048]{2,1,0:T(8,128)(2,1)}, u32[]{:S(2)}, u32[]{:S(2)}) async-start(bf16[16,32,2048]{2,1,0:T(8,128)(2,1)} %reduce-scatter.5.cloned.1.call-done), calls=%async_computation.3 | async-start | bytes 4194304 | tf_op jit(solution)/shard_map/all_to_all | solution.py:187
  329.8 14.5 %copy-start.1 = (bf16[512,2048]{1,0:T(8,128)(2,1)S(1)}, bf16[512,2048]{1,0:T(8,128)(2,1)}, u32[]{:S(2)}) copy-start(bf16[512,2048]{1,0:T(8,128)(2,1)} %param.24) | copy-start | bytes 6291460
  335.0 8.3 %copy-start.3 = (bf16[128,2048]{1,0:T(8,128)(2,1)S(1)}, bf16[128,2048]{1,0:T(8,128)(2,1)}, u32[]{:S(2)}) copy-start(bf16[128,2048]{1,0:T(8,128)(2,1)} %reduce-scatter.3.cloned.1.call-done) | copy-start | bytes 1572868
Sparse Core Ops, SparseCore 0:
  17.7 60.4 all-gather.6
  104.8 16.9 reduce-scatter.2
  214.4 13.8 all-gather.4
  261.0 13.3 reduce-scatter.4
where the time goes:
time: 353 us; the launch traced here: 351 us
  waiting for transfers between devices  115 us (33%)
  blocking collectives  82.2 us (23%)
  local copies, waits for them, and re-layouts  61.7 us (17%)
  matrix products  44.3 us (13%)
  other arithmetic  26.3 us (7%)
  between operations  13.4 us (4%)
  starting transfers between devices  7.27 us (2%)
    all_to_all x1, blocking collectives, shards(): lax.all_to_all(outgoing, 'sp', split_axis=0, concat_axis=0, tiled=True)  54 us
    all_to_all x1, waiting for transfers between devices, shards(): lax.all_to_all(summed, 'sp', split_axis=0, concat_axis=0, tiled=True)  48.3 us
    scatter x1, local copies, waits for them, and re-layouts, shards(): outgoing = jnp.zeros((experts, capacity, d_model), jnp.bfloat16).at[flat_...  33.3 us
    all_gather x1, blocking collectives, prefix(): lax.all_gather(a.astype(kind), axis)  28.1 us
    all_gather x1, waiting for transfers between devices, prefix(): lax.all_gather(a.astype(kind), axis)  24.1 us
    reduce_scatter x1, waiting for transfers between devices, shards(): lax.psum_scatter(jnp.dot(normed, out_weight, preferred_element_type=jnp.f...  15.5 us
    all_gather x1, waiting for transfers between devices, shards(): lax.all_gather(lax.all_to_all(outgoing, 'sp', split_axis=0, concat_axis=0...  13.8 us
    reduce_scatter x1, waiting for transfers between devices, shards(): lax.psum_scatter(partial_value.reshape(both_halves.shape).astype(jnp.bflo...  13.5 us
  transfers between devices with their start and end apart: 5, of which 5 were waited for; matrix products, arithmetic and copies ran while one was open for 3% of the time, Pallas kernels for 0%

commit v1 on v0

v1 whole, which is shorter than its diff:
```python
import jax
import jax.numpy as jnp
from jax import lax
from jax.sharding import PartitionSpec as P


def swap(value):
    return lax.ppermute(value, "tp", [(0, 1), (1, 0)])


def incoming_state(total, state):
    heads, size, _ = state.shape
    count = lax.axis_size("sp")
    state = jnp.swapaxes(state, 0, 1).reshape(size, heads * size)
    total = jnp.repeat(total, size)[None, :]

    def shift(total, state, distance):
        high = total.astype(jnp.bfloat16)
        low = (total - high.astype(jnp.float32)).astype(jnp.bfloat16)
        packed = jnp.concatenate([state.astype(jnp.bfloat16), high, low], axis=0)
        got = lax.ppermute(packed, "sp", [(i, i + distance) for i in range(count - distance)])
        got = got.astype(jnp.float32)
        return got[size : size + 1] + got[size + 1 : size + 2], got[:size]

    total, state = shift(total, state, 1)
    distance = 1
    while distance < count:
        earlier_total, earlier_state = shift(total, state, distance)
        state = jnp.exp(total) * earlier_state + state
        total = total + earlier_total
        distance *= 2
    return jnp.swapaxes(state.reshape(size, heads, size), 0, 1)


def rotate(block, places):
    half_size = block.shape[-1] // 2
    frequency = 10000.0 ** (-jnp.arange(half_size, dtype=jnp.float32) / half_size)
    angles = places.astype(jnp.float32)[:, None, None] * frequency
    first_half = block[..., :half_size]
    second = block[..., half_size:]
    return jnp.concatenate(
        [
            first_half * jnp.cos(angles) - second * jnp.sin(angles),
            second * jnp.cos(angles) + first_half * jnp.sin(angles),
        ],
        axis=-1,
    )


def expert_hidden(batch, gate_matrix, up_matrix):
    gate_value = jnp.dot(batch, gate_matrix, preferred_element_type=jnp.float32)
    up_value = jnp.dot(batch, up_matrix, preferred_element_type=jnp.float32)
    return (jax.nn.silu(gate_value) * up_value).astype(jnp.bfloat16)


def shards(
    queries,
    key_vectors,
    value_vectors,
    gate_inputs,
    log_decay,
    head_gain,
    out_weight,
    residual,
    norm_gain,
    expert_ids,
    expert_weights,
    gate_experts,
    up_experts,
    down_experts,
):
    tok_dev, channels = queries.shape
    head_count = log_decay.shape[1]
    head_size = channels // head_count
    places = lax.axis_index("sp") * tok_dev + jnp.arange(tok_dev, dtype=jnp.int32)
    core = lax.axis_index("tp")
    turned_queries = rotate(
        queries.astype(jnp.float32).reshape(tok_dev, head_count, head_size), places
    )
    turned_keys = rotate(
        key_vectors.astype(jnp.float32).reshape(tok_dev, head_count, head_size), places
    ) * head_size ** (-0.5)
    value_float = value_vectors.astype(jnp.float32).reshape(tok_dev, head_count, head_size)
    running = jnp.cumsum(log_decay, axis=0)
    device_total = running[-1]
    end_weight = jnp.exp(device_total[None, :] - running)
    local_end = jnp.einsum(
        "thd,the->hde",
        turned_keys * end_weight[:, :, None],
        value_float,
        precision=lax.Precision.HIGH,
    )
    incoming = incoming_state(device_total, local_end)
    by_head = running.T
    log_gaps = by_head[:, :, None] - by_head[:, None, :]
    offsets = jnp.arange(tok_dev)
    causal = offsets[:, None] >= offsets[None, :]
    decay_weight = jnp.where(causal, jnp.exp(jnp.where(causal, log_gaps, 0.0)), 0.0)
    scores = (
        jnp.einsum("thd,shd->hts", turned_queries, turned_keys, precision=lax.Precision.HIGH)
        * decay_weight
    )
    within = jnp.einsum("hts,she->the", scores, value_float, precision=lax.Precision.HIGH)
    carried = jnp.einsum(
        "thd,hde->the",
        turned_queries * jnp.exp(running)[:, :, None],
        incoming,
        precision=lax.Precision.HIGH,
    )
    retained = within + carried
    squares = jnp.mean(retained * retained, axis=-1, keepdims=True)
    normed = retained * lax.rsqrt(squares + 1e-06) * head_gain.reshape(head_count, head_size)
    normed = (
        normed.reshape(tok_dev, channels) * jax.nn.silu(gate_inputs.astype(jnp.float32))
    ).astype(jnp.bfloat16)
    half = tok_dev // 2
    normed_away = lax.dynamic_slice_in_dim(normed, (1 - core) * half, half, 0)
    normed_here = lax.dynamic_slice_in_dim(normed, core * half, half, 0)
    away = jnp.dot(normed_away, out_weight, preferred_element_type=jnp.float32)
    got = swap(away.astype(jnp.bfloat16))
    here = jnp.dot(normed_here, out_weight, preferred_element_type=jnp.float32)
    projected = here.astype(jnp.bfloat16).astype(jnp.float32) + got.astype(jnp.float32)
    mixed_rows = (residual.astype(jnp.float32) + projected).astype(jnp.bfloat16)
    mixed_float = mixed_rows.astype(jnp.float32)
    normed_rows = (
        mixed_float
        * lax.rsqrt(jnp.mean(mixed_float * mixed_float, axis=-1, keepdims=True) + 1e-06)
        * norm_gain
    ).astype(jnp.bfloat16)
    d_model = residual.shape[1]
    experts = lax.axis_size("sp")
    capacity = 2 * tok_dev // experts
    slots = experts * capacity
    top_count = expert_ids.shape[1]
    flat_routes = expert_ids.reshape(-1)
    onehot = (flat_routes[:, None] == jnp.arange(experts, dtype=jnp.int32)[None, :]).astype(
        jnp.int32
    )
    slot_rank = jnp.sum(jnp.cumsum(onehot, axis=0) * onehot, axis=1) - 1
    slot = (flat_routes * capacity + slot_rank).reshape(-1, top_count)
    every_slot = jnp.arange(slots, dtype=jnp.int32)
    place = jnp.zeros((slots, half), jnp.bool_)
    weigh = jnp.zeros((half, slots), jnp.float32)
    for choice in range(top_count):
        column = slot[:, choice]
        place = place | (every_slot[:, None] == column[None, :])
        weigh = weigh + jnp.where(
            column[:, None] == every_slot[None, :], expert_weights[:, choice][:, None], 0.0
        )
    outgoing = jnp.dot(
        place.astype(jnp.bfloat16), normed_rows, preferred_element_type=jnp.float32
    ).astype(jnp.bfloat16)
    arrived = lax.all_to_all(
        outgoing.reshape(experts, capacity, d_model), "sp", split_axis=0, concat_axis=0, tiled=True
    ).reshape(slots, d_model)
    partner = swap(arrived)
    hidden_here = expert_hidden(arrived, gate_experts[0], up_experts[0])
    hidden_away = expert_hidden(partner, gate_experts[0], up_experts[0])
    part_away = jnp.dot(hidden_away, down_experts[0], preferred_element_type=jnp.float32)
    got_part = swap(part_away.astype(jnp.bfloat16))
    part_here = jnp.dot(hidden_here, down_experts[0], preferred_element_type=jnp.float32)
    summed = (
        part_here.astype(jnp.bfloat16).astype(jnp.float32) + got_part.astype(jnp.float32)
    ).astype(jnp.bfloat16)
    returned = lax.all_to_all(
        summed.reshape(experts, capacity, d_model), "sp", split_axis=0, concat_axis=0, tiled=True
    ).reshape(slots, d_model)
    weigh_high = weigh.astype(jnp.bfloat16)
    weigh_low = (weigh - weigh_high.astype(jnp.float32)).astype(jnp.bfloat16)
    expert_sum = jnp.dot(weigh_high, returned, preferred_element_type=jnp.float32) + jnp.dot(
        weigh_low, returned, preferred_element_type=jnp.float32
    )
    return (mixed_float + expert_sum).astype(jnp.bfloat16)


def solution(mesh):
    return jax.shard_map(
        shards,
        mesh=mesh,
        in_specs=(
            P("sp", "tp"),
            P("sp", "tp"),
            P("sp", "tp"),
            P("sp", "tp"),
            P("sp", "tp"),
            P("tp"),
            P("tp", None),
            P(("sp", "tp"), None),
            P(),
            P(("sp", "tp"), None),
            P(("sp", "tp"), None),
            P("sp", None, "tp"),
            P("sp", None, "tp"),
            P("sp", "tp", None),
        ),
        out_specs=P(("sp", "tp"), None),
        check_vma=False,
    )
```

time: 353 us -> 234 us (0.66)
  local copies, waits for them, and re-layouts: 61.7 us -> 9.12 us
  waiting for transfers between devices: 115 us -> 63.9 us
  blocking collectives: 82.2 us -> 57.9 us
  matrix products: 44.3 us -> 64.8 us
  starting transfers between devices: 7.27 us -> 25.1 us
  other arithmetic: 26.3 us -> 12.3 us
  between operations: 13.4 us -> 0.44 us
    all_gather x2 -> x0, waiting for transfers between devices: 37.9 us -> none  [the longest x1 24.1 us: prefix(): lax.all_gather(a.astype(kind), axis)]
    scatter x1 -> x0, local copies, waits for them, and re-layouts: 33.3 us -> none  [shards(): outgoing = jnp.zeros((experts, capacity, d_model), jnp.bfloat16).at[flat_...]
    reduce_scatter x2 -> x0, waiting for transfers between devices: 29 us -> none  [the longest x1 15.5 us: shards(): lax.psum_scatter(jnp.dot(normed, out_weight, preferred_element_type=jnp.f...]
    all_gather x1 -> x0, blocking collectives: 28.1 us -> none  [prefix(): lax.all_gather(a.astype(kind), axis)]
    dot_general x10, matrix products: 19.1 us -> 45.9 us  [the longest x1 17.6 us: shards(): jnp.dot(hidden_here, down_experts[0], preferred_element_type=jnp.float32)]
    ppermute x0 -> x8, starting transfers between devices: none -> 18.6 us  [the longest x5 18.4 us: shift(): lax.ppermute(packed, 'sp', [(i, i + distance) for i in range(count - dist...]
    ppermute x0 -> x8, waiting for transfers between devices: none -> 14.6 us  [the longest x5 8.61 us: shift(): lax.ppermute(packed, 'sp', [(i, i + distance) for i in range(count - dist...]
    gather x2 -> x0, local copies, waits for them, and re-layouts: 7.55 us -> none  [the longest x1 5.2 us: shards(): returned[flat_routes, slot_rank].astype(jnp.float32)]
  transfers between devices with their start and end apart: 5 -> 9, of which waited for: 5 -> 7; matrix products, arithmetic and copies ran while one was open for 3% -> 6% of each run, Pallas kernels for 0% -> 0%
where the time goes in v1:
time: 234 us
  matrix products  64.8 us (28%)
  waiting for transfers between devices  63.9 us (27%)
  blocking collectives  57.9 us (25%)
  starting transfers between devices  25.1 us (11%)
  other arithmetic  12.3 us (5%)
  local copies, waits for them, and re-layouts  9.12 us (4%)
    all_to_all x1, blocking collectives, shards(): lax.all_to_all(outgoing.reshape(experts, capacity, d_model), 'sp', split_...  57.9 us
    all_to_all x1, waiting for transfers between devices, shards(): lax.all_to_all(summed.reshape(experts, capacity, d_model), 'sp', split_ax...  49.4 us
    ppermute x5, starting transfers between devices, shift(): lax.ppermute(packed, 'sp', [(i, i + distance) for i in range(count - dist...  18.4 us
    dot_general x1, matrix products, shards(): jnp.dot(hidden_here, down_experts[0], preferred_element_type=jnp.float32)  17.6 us
    dot_general x1, matrix products, shards(): jnp.dot(hidden_away, down_experts[0], preferred_element_type=jnp.float32)  17 us
    dot_general x1, matrix products, expert_hidden(): gate_value = jnp.dot(batch, gate_matrix, preferred_element_type=jnp.float32)  9.7 us
    dot_general x1, matrix products, expert_hidden(): up_value = jnp.dot(batch, up_matrix, preferred_element_type=jnp.float32)  8.86 us
    ppermute x5, waiting for transfers between devices, shift(): lax.ppermute(packed, 'sp', [(i, i + distance) for i in range(count - dist...  8.61 us
  transfers between devices with their start and end apart: 9, of which 7 were waited for; matrix products, arithmetic and copies ran while one was open for 6% of the time, Pallas kernels for 0%

profile of v1, /device:TPU:14, one launch (start us, length us, event | category | flops | bytes accessed | tf_op | source)
XLA Modules:
  0.0 233.6 jit_solution(4472569699401480527)
XLA Ops:
  0.0 1.4 reduce-window.14
  1.4 0.2 slice_reduce_fusion.1
  1.7 0.2 slice_reduce_fusion.2
  1.9 0.1 exponential_multiply_fusion
  2.0 1.1 copy.48
  3.1 0.8 convert.3
  3.9 1.1 copy.49
  5.0 0.8 convert.4
  5.8 0.1 copy.50
  6.0 0.2 multiply_cosine_fusion
  6.2 1.3 multiply_subtract_fusion.1
  7.5 0.3 fusion.40
  7.8 0.1 copy.51
  7.9 0.8 convert_element_type.194
  8.7 0.7 broadcast_in_dim.57
  9.4 0.1 broadcast_in_dim_reshape.2
  9.5 0.9 pad_maximum_fusion.6
  10.4 3.4 %collective-permute-start = (bf16[66,512]{1,0:T(8,128)(2,1)S(1)}, bf16[66,512]{1,0:T(8,128)(2,1)S(1)}, u32[]{:S(2)}, u32[]{:S(2)}) collective-permute-start(bf16[66,512]{1,0:T(8,128)(2,1)S(1)} %pad_maximum_fusion.6), channel_id=1, source_target_pairs={{0,2},{2,4},{4,6},{6,8},{8,10},{10,12},{12,14},{14,16},{16,18},{18... | collective-permute-start | bytes 202760 | tf_op jit(solution)/shard_map/ppermute | solution.py:21
  13.8 0.7 add_bitcast_fusion.2
  14.5 1.0 fusion.59
  15.6 1.0 collective-permute-done
  16.7 0.6 pad_maximum_fusion.7
  17.3 5.3 %collective-permute-start.1 = (bf16[66,512]{1,0:T(8,128)(2,1)}, bf16[66,512]{1,0:T(8,128)(2,1)S(1)}, u32[]{:S(2)}, u32[]{:S(2)}) collective-permute-start(bf16[66,512]{1,0:T(8,128)(2,1)} %pad_maximum_fusion.7), channel_id=1, source_target_pairs={{0,2},{2,4},{4,6},{6,8},{8,10},{10,12},{12,14},{14,16},{16,18},{18... | collective-permute-start | bytes 202760 | tf_op jit(solution)/shard_map/ppermute | solution.py:21
  22.6 2.0 fusion.36
  24.6 0.1 copy.54
  24.7 0.1 eq.85
  25.0 2.7 %collective-permute-start.2 = (bf16[66,512]{1,0:T(8,128)(2,1)S(1)}, bf16[66,512]{1,0:T(8,128)(2,1)}, u32[]{:S(2)}, u32[]{:S(2)}) collective-permute-start(bf16[66,512]{1,0:T(8,128)(2,1)S(1)} %pad_maximum_fusion.8), channel_id=1, source_target_pairs={{0,4},{2,6},{4,8},{6,10},{8,12},{10,14},{12,16},{14,18},{16,20},{1... | collective-permute-start | bytes 202760 | tf_op jit(solution)/shard_map/ppermute | solution.py:21
  27.8 0.1 eq.81
  27.9 0.1 mul.266
  28.0 0.6 reduce-window.16
  28.5 2.8 %collective-permute-done.2 = bf16[66,512]{1,0:T(8,128)(2,1)} collective-permute-done((bf16[66,512]{1,0:T(8,128)(2,1)S(1)}, bf16[66,512]{1,0:T(8,128)(2,1)}, u32[]{:S(2)}, u32[]{:S(2)}) %collective-permute-start.2) | collective-permute-done | bytes 67616 | tf_op jit(solution)/shard_map/ppermute | solution.py:21
  31.4 0.9 convert_element_type.208
  32.3 0.6 pad_maximum_fusion.9
  33.0 3.5 %collective-permute-start.3 = (bf16[66,512]{1,0:T(8,128)(2,1)}, bf16[66,512]{1,0:T(8,128)(2,1)}, u32[]{:S(2)}, u32[]{:S(2)}) collective-permute-start(bf16[66,512]{1,0:T(8,128)(2,1)} %pad_maximum_fusion.9), channel_id=1, source_target_pairs={{0,8},{2,10},{4,12},{6,14},{8,16},{10,18},{12,20},{14,22},{16,24},... | collective-permute-start | bytes 202760 | tf_op jit(solution)/shard_map/ppermute | solution.py:21
  36.4 0.2 slice_reduce_fusion
  36.7 2.8 %collective-permute-done.3 = bf16[66,512]{1,0:T(8,128)(2,1)} collective-permute-done((bf16[66,512]{1,0:T(8,128)(2,1)}, bf16[66,512]{1,0:T(8,128)(2,1)}, u32[]{:S(2)}, u32[]{:S(2)}) %collective-permute-start.3) | collective-permute-done | bytes 67616 | tf_op jit(solution)/shard_map/ppermute | solution.py:21
  39.5 0.9 convert_element_type.213
  40.5 3.5 %collective-permute-start.4 = (bf16[66,512]{1,0:T(8,128)(2,1)S(1)}, bf16[66,512]{1,0:T(8,128)(2,1)S(1)}, u32[]{:S(2)}, u32[]{:S(2)}) collective-permute-start(bf16[66,512]{1,0:T(8,128)(2,1)S(1)} %pad_maximum_fusion.10), channel_id=1, source_target_pairs={{0,16},{2,18},{4,20},{6,22},{8,24},{10,26},{12,28},{14,30},{1,17},... | collective-permute-start | bytes 202760 | tf_op jit(solution)/shard_map/ppermute | solution.py:21
  44.0 0.1 fusion.87
  44.1 1.9 collective-permute-done.4
  46.0 0.7 multiply_add_fusion.2
  46.6 1.0 copy.58
  47.7 0.4 multiply_reduce_fusion
  48.1 0.1 multiply_multiply_fusion
  48.2 0.2 copy.53
  48.4 1.1 fusion.61
  49.6 0.4 convolution_convert_fusion.1
  50.1 0.1 sub.79
  50.4 1.8 collective-permute-done.5
  52.1 1.7 fusion.43
  53.9 0.8 convolution_convert_fusion
  54.7 57.9 %all_to_all.10 = bf16[16,32,2048]{2,1,0:T(8,128)(2,1)S(1)} all-to-all(bf16[16,32,2048]{2,1,0:T(8,128)(2,1)S(1)} %bitcast.97), channel_id=1, replica_groups=mesh['sp'=16,'tp'=2] {'sp'}, dimensions={0} | all-to-all | bytes 4194304 | tf_op jit(solution)/shard_map/all_to_all | solution.py:153
  112.6 1.3 copy-done.1
  113.9 4.2 %collective-permute-done.6 = bf16[512,2048]{1,0:T(8,128)(2,1)S(1)} collective-permute-done((bf16[512,2048]{1,0:T(8,128)(2,1)S(1)}, bf16[512,2048]{1,0:T(8,128)(2,1)S(1)}, u32[]{:S(2)}, u32[]{:S(2)}) %collective-permute-start.6) | collective-permute-done | bytes 2097184 | tf_op jit(solution)/shard_map/ppermute | solution.py:8
  118.1 1.4 copy-done.11
  119.5 8.9 %fusion.4 = f32[512,1792]{1,0:T(8,128)} fusion(bf16[512,2048]{1,0:T(8,128)(2,1)S(1)} %collective-permute-done.6, bf16[1,2048,1792]{2,1,0:T(8,128)(2,1)} %param.26), kind=kOutput, calls=%fused_computation.4 | convolution fusion | flops 3758096384 | bytes 13107200 | tf_op jit(solution)/shard_map/dot_general | solution.py:52
  128.3 17.0 %fusion.17 = bf16[512,2048]{1,0:T(8,128)(2,1)} fusion(bf16[1,1792,2048]{2,1,0:T(8,128)(2,1)} %param.27, f32[512,1792]{1,0:T(8,128)} %fusion.4, bf16[512,2048]{1,0:T(8,128)(2,1)} %copy-done.11, bf16[1,2048,1792]{2,1,0:T(8,128)(2,1)} %param.25), kind=kOutput, calls=%fused_computation.16 | convolution fusion | flops 7522746368 | bytes 22544384 | tf_op jit(solution)/shard_map/dot_general | solution.py:159
  145.3 0.1 collective-permute-start.7
  145.4 9.7 %fusion.10 = f32[512,1792]{1,0:T(8,128)} fusion(bf16[512,2048]{1,0:T(8,128)(2,1)} %bitcast.99, bf16[1,2048,1792]{2,1,0:T(8,128)(2,1)} %param.25), kind=kOutput, calls=%fused_computation.10 | convolution fusion | flops 3758096384 | bytes 13107200 | tf_op jit(solution)/shard_map/dot_general | solution.py:51
  155.1 17.6 %add_convert_fusion = bf16[512,2048]{1,0:T(8,128)(2,1)} fusion(bf16[512,2048]{1,0:T(8,128)(2,1)} %collective-permute-done.7, bf16[1,1792,2048]{2,1,0:T(8,128)(2,1)} %param.27, f32[512,1792]{1,0:T(8,128)} %fusion.10, bf16[512,2048]{1,0:T(8,128)(2,1)} %bitcast.100, bf16[1,2048,1792]{2,1,0:T(8,128)(2,1)} %param.26), kind=kOutput, calls=%fused_computation.12 | convolution fusion | flops 7526940672 | bytes 24641536 | tf_op jit(solution)/shard_map/dot_general | solution.py:161
  172.7 6.5 %all-to-all-start.1 = ((bf16[16,32,2048]{2,1,0:T(8,128)(2,1)}), bf16[16,32,2048]{2,1,0:T(8,128)(2,1)}, u32[]{:S(2)}, u32[]{:S(2)}) async-start(bf16[16,32,2048]{2,1,0:T(8,128)(2,1)} %bitcast.101), calls=%async_computation.1 | async-start | bytes 4194304 | tf_op jit(solution)/shard_map/all_to_all | solution.py:165
  179.2 49.4 %all-to-all-done.1 = bf16[16,32,2048]{2,1,0:T(8,128)(2,1)} async-done(((bf16[16,32,2048]{2,1,0:T(8,128)(2,1)}), bf16[16,32,2048]{2,1,0:T(8,128)(2,1)}, u32[]{:S(2)}, u32[]{:S(2)}) %all-to-all-start.1) | async-done | bytes 2097184 | tf_op jit(solution)/shard_map/all_to_all | solution.py:165
  228.6 2.1 fusion.83
  230.7 2.9 %fusion.23 = bf16[128,2048]{1,0:T(8,128)(2,1)} fusion(f32[128,2048]{1,0:T(8,128)S(1)} %fusion.83, bf16[512,2048]{1,0:T(8,128)(2,1)} %bitcast.31, bf16[128,2048]{1,0:T(8,128)(2,1)S(1)} %get-tuple-element.44, f32[128]{0:T(128)S(1)} %get-tuple-element.38, s32[128]{0:T(128)S(1)} %get-tuple-element.40, f32[128]{0:T(128)S(1)} %get-tuple-element.37, ...), kind=kOutput, calls=%fused_computation.20 | convolution fusion | flops 270073856 | bytes 4196352 | tf_op jit(solution)/shard_map/dot_general | solution.py:170
  (59 shorter events, 0.7 us)
Async XLA Ops:
  0.0 49.5 %copy-start = (bf16[512,2048]{1,0:T(8,128)(2,1)S(1)}, bf16[512,2048]{1,0:T(8,128)(2,1)}, u32[]{:S(2)}) copy-start(bf16[512,2048]{1,0:T(8,128)(2,1)} %param.20) | copy-start | bytes 6291460
  0.0 5.8 %copy-start.4 = (bf16[256,512]{1,0:T(8,128)(2,1)S(1)}, bf16[256,512]{1,0:T(8,128)(2,1)}, u32[]{:S(2)}) copy-start(bf16[256,512]{1,0:T(8,128)(2,1)} %param.16) | copy-start | bytes 786436
  1.6 4.5 %copy-start.5 = (f32[8,2]{0,1:T(2,128)}, f32[8,2]{0,1:T(2,128)S(1)}, u32[]{:S(2)}) copy-start(f32[8,2]{0,1:T(2,128)S(1)} %slice.86) | copy-start | bytes 196
  1.9 5.6 %copy-start.7 = (f32[8]{0:T(128)}, f32[8]{0:T(128)S(1)}, u32[]{:S(2)}) copy-start(f32[8]{0:T(128)S(1)} %slice_reduce_fusion.2) | copy-start | bytes 100
  10.4 6.2 %collective-permute-start = (bf16[66,512]{1,0:T(8,128)(2,1)S(1)}, bf16[66,512]{1,0:T(8,128)(2,1)S(1)}, u32[]{:S(2)}, u32[]{:S(2)}) collective-permute-start(bf16[66,512]{1,0:T(8,128)(2,1)S(1)} %pad_maximum_fusion.6), channel_id=1, source_target_pairs={{0,2},{2,4},{4,6},{6,8},{8,10},{10,12},{12,14},{14,16},{16,18},{18... | collective-permute-start | bytes 202760 | tf_op jit(solution)/shard_map/ppermute | solution.py:21
  17.3 7.3 %copy-start.8 = (s32[128,2]{0,1:T(2,128)S(1)}, s32[128,2]{0,1:T(2,128)}, u32[]{:S(2)}) copy-start(s32[128,2]{0,1:T(2,128)} %param.23) | copy-start | bytes 3076
  17.3 10.6 %copy-start.9 = (f32[512]{0:T(512)S(1)}, f32[512]{0:T(512)}, u32[]{:S(2)}) copy-start(f32[512]{0:T(512)} %param.19) | copy-start | bytes 6148
  17.3 7.6 %collective-permute-start.1 = (bf16[66,512]{1,0:T(8,128)(2,1)}, bf16[66,512]{1,0:T(8,128)(2,1)S(1)}, u32[]{:S(2)}, u32[]{:S(2)}) collective-permute-start(bf16[66,512]{1,0:T(8,128)(2,1)} %pad_maximum_fusion.7), channel_id=1, source_target_pairs={{0,2},{2,4},{4,6},{6,8},{8,10},{10,12},{12,14},{14,16},{16,18},{18... | collective-permute-start | bytes 202760 | tf_op jit(solution)/shard_map/ppermute | solution.py:21
  24.6 23.0 %copy-start.2 = (f32[256,8,64]{0,2,1:T(8,128)S(1)}, f32[256,8,64]{0,2,1:T(8,128)}, u32[]{:S(2)}) copy-start(f32[256,8,64]{0,2,1:T(8,128)} %fusion.36) | copy-start | bytes 1572868
  25.0 6.4 %collective-permute-start.2 = (bf16[66,512]{1,0:T(8,128)(2,1)S(1)}, bf16[66,512]{1,0:T(8,128)(2,1)}, u32[]{:S(2)}, u32[]{:S(2)}) collective-permute-start(bf16[66,512]{1,0:T(8,128)(2,1)S(1)} %pad_maximum_fusion.8), channel_id=1, source_target_pairs={{0,4},{2,6},{4,8},{6,10},{8,12},{10,14},{12,16},{14,18},{16,20},{1... | collective-permute-start | bytes 202760 | tf_op jit(solution)/shard_map/ppermute | solution.py:21
  33.0 6.6 %collective-permute-start.3 = (bf16[66,512]{1,0:T(8,128)(2,1)}, bf16[66,512]{1,0:T(8,128)(2,1)}, u32[]{:S(2)}, u32[]{:S(2)}) collective-permute-start(bf16[66,512]{1,0:T(8,128)(2,1)} %pad_maximum_fusion.9), channel_id=1, source_target_pairs={{0,8},{2,10},{4,12},{6,14},{8,16},{10,18},{12,20},{14,22},{16,24},... | collective-permute-start | bytes 202760 | tf_op jit(solution)/shard_map/ppermute | solution.py:21
  40.5 5.4 %collective-permute-start.4 = (bf16[66,512]{1,0:T(8,128)(2,1)S(1)}, bf16[66,512]{1,0:T(8,128)(2,1)S(1)}, u32[]{:S(2)}, u32[]{:S(2)}) collective-permute-start(bf16[66,512]{1,0:T(8,128)(2,1)S(1)} %pad_maximum_fusion.10), channel_id=1, source_target_pairs={{0,16},{2,18},{4,20},{6,22},{8,24},{10,26},{12,28},{14,30},{1,17},... | collective-permute-start | bytes 202760 | tf_op jit(solution)/shard_map/ppermute | solution.py:21
  49.5 2.6 %copy-start.3 = (bf16[128,2048]{1,0:T(8,128)(2,1)S(1)}, bf16[128,2048]{1,0:T(8,128)(2,1)}, u32[]{:S(2)}) copy-start(bf16[128,2048]{1,0:T(8,128)(2,1)} %param.21) | copy-start | bytes 1572868
  50.0 3.8 %copy-start.6 = (f32[2048]{0:T(1024)S(1)}, f32[2048]{0:T(1024)}, u32[]{:S(2)}) copy-start(f32[2048]{0:T(1024)} %param.22) | copy-start | bytes 24580
  50.0 2.1 collective-permute-start.5
  112.6 1.3 copy-start.1
  113.9 4.2 %collective-permute-start.6 = (bf16[512,2048]{1,0:T(8,128)(2,1)S(1)}, bf16[512,2048]{1,0:T(8,128)(2,1)S(1)}, u32[]{:S(2)}, u32[]{:S(2)}) collective-permute-start(bf16[512,2048]{1,0:T(8,128)(2,1)S(1)} %bitcast.98), channel_id=1, source_target_pairs={{0,1},{1,0},{2,3},{3,2},{4,5},{5,4},{6,7},{7,6},{8,9},{9,8},{10,11... | collective-permute-start | bytes 6291464 | tf_op jit(solution)/shard_map/ppermute | solution.py:8
  118.1 1.4 copy-start.11
  145.3 9.8 %collective-permute-start.7 = (bf16[512,2048]{1,0:T(8,128)(2,1)}, bf16[512,2048]{1,0:T(8,128)(2,1)}, u32[]{:S(2)}, u32[]{:S(2)}) collective-permute-start(bf16[512,2048]{1,0:T(8,128)(2,1)} %fusion.17), channel_id=1, source_target_pairs={{0,1},{1,0},{2,3},{3,2},{4,5},{5,4},{6,7},{7,6},{8,9},{9,8},{10,11... | collective-permute-start | bytes 6291464 | tf_op jit(solution)/shard_map/ppermute | solution.py:8
  172.7 6.5 %copy-start.10 = (f32[128,2]{0,1:T(2,128)S(1)}, f32[128,2]{0,1:T(2,128)}, u32[]{:S(2)}) copy-start(f32[128,2]{0,1:T(2,128)} %param.24) | copy-start | bytes 3076
  172.7 55.9 %all-to-all-start.1 = ((bf16[16,32,2048]{2,1,0:T(8,128)(2,1)}), bf16[16,32,2048]{2,1,0:T(8,128)(2,1)}, u32[]{:S(2)}, u32[]{:S(2)}) async-start(bf16[16,32,2048]{2,1,0:T(8,128)(2,1)} %bitcast.101), calls=%async_computation.1 | async-start | bytes 4194304 | tf_op jit(solution)/shard_map/all_to_all | solution.py:165

commit v2 on v1

--- a/solution.py
+++ b/solution.py
@@ -22,14 +22,16 @@
         got = got.astype(jnp.float32)
         return got[size : size + 1] + got[size + 1 : size + 2], got[:size]
 
-    total, state = shift(total, state, 1)
+    before_total, before_state = jnp.zeros_like(total), jnp.zeros_like(state)
     distance = 1
     while distance < count:
         earlier_total, earlier_state = shift(total, state, distance)
+        before_state = jnp.exp(before_total) * earlier_state + before_state
+        before_total = before_total + earlier_total
         state = jnp.exp(total) * earlier_state + state
         total = total + earlier_total
         distance *= 2
-    return jnp.swapaxes(state.reshape(size, heads, size), 0, 1)
+    return jnp.swapaxes(before_state.reshape(size, heads, size), 0, 1)
 
 
 def rotate(block, places):
@@ -153,14 +155,15 @@
     arrived = lax.all_to_all(
         outgoing.reshape(experts, capacity, d_model), "sp", split_axis=0, concat_axis=0, tiled=True
     ).reshape(slots, d_model)
-    partner = swap(arrived)
-    hidden_here = expert_hidden(arrived, gate_experts[0], up_experts[0])
-    hidden_away = expert_hidden(partner, gate_experts[0], up_experts[0])
-    part_away = jnp.dot(hidden_away, down_experts[0], preferred_element_type=jnp.float32)
-    got_part = swap(part_away.astype(jnp.bfloat16))
-    part_here = jnp.dot(hidden_here, down_experts[0], preferred_element_type=jnp.float32)
+    both = jnp.concatenate([swap(arrived), arrived], axis=0)
+    hidden = expert_hidden(both, gate_experts[0], up_experts[0])
+    part = jnp.dot(hidden, down_experts[0], preferred_element_type=jnp.float32).astype(
+        jnp.bfloat16
+    )
+    got_part = swap(part[:slots])
+    part_here = part[slots:]
     summed = (
-        part_here.astype(jnp.bfloat16).astype(jnp.float32) + got_part.astype(jnp.float32)
+        part_here.astype(jnp.float32) + got_part.astype(jnp.float32)
     ).astype(jnp.bfloat16)
     returned = lax.all_to_all(
         summed.reshape(experts, capacity, d_model), "sp", split_axis=0, concat_axis=0, tiled=True

time: 234 us -> 206 us (0.88)
  matrix products: 64.8 us -> 46.7 us
  starting transfers between devices: 25.1 us -> 19.9 us
    dot_general x2 -> x1, matrix products: 34.5 us -> 10.6 us  [shards(): jnp.dot(hidden, down_experts[0], preferred_element_type=jnp.float32)]
    ppermute x5 -> x4, starting transfers between devices: 18.4 us -> 13.3 us  [shift(): lax.ppermute(packed, 'sp', [(i, i + distance) for i in range(count - dist...]
    ppermute x3, waiting for transfers between devices: 5.95 us -> 9.82 us  [swap(): return lax.ppermute(value, 'tp', [(0, 1), (1, 0)])]
    dot_general x1, matrix products: 8.86 us -> 11.4 us  [expert_hidden(): up_value = jnp.dot(batch, up_matrix, preferred_element_type=jnp.float32)]
    ppermute x5 -> x4, waiting for transfers between devices: 8.61 us -> 6.41 us  [shift(): lax.ppermute(packed, 'sp', [(i, i + distance) for i in range(count - dist...]
    unnamed x28 -> x32, local copies, waits for them, and re-layouts: 5.16 us -> 3.94 us
  transfers between devices with their start and end apart: 9 -> 8, of which waited for: 7 -> 7; matrix products, arithmetic and copies ran while one was open for 6% -> 3% of each run, Pallas kernels for 0% -> 0%
where the time goes in v2:
time: 206 us
  waiting for transfers between devices  65 us (32%)
  blocking collectives  56.8 us (28%)
  matrix products  46.7 us (23%)
  starting transfers between devices  19.9 us (10%)
  other arithmetic  9.98 us (5%)
  local copies, waits for them, and re-layouts  6.8 us (3%)
    all_to_all x1, blocking collectives, shards(): lax.all_to_all(outgoing.reshape(experts, capacity, d_model), 'sp', split_...  56.8 us
    all_to_all x1, waiting for transfers between devices, shards(): lax.all_to_all(summed.reshape(experts, capacity, d_model), 'sp', split_ax...  48.7 us
    ppermute x4, starting transfers between devices, shift(): lax.ppermute(packed, 'sp', [(i, i + distance) for i in range(count - dist...  13.3 us
    dot_general x1, matrix products, expert_hidden(): up_value = jnp.dot(batch, up_matrix, preferred_element_type=jnp.float32)  11.4 us
    dot_general x1, matrix products, expert_hidden(): gate_value = jnp.dot(batch, gate_matrix, preferred_element_type=jnp.float32)  11 us
    dot_general x1, matrix products, shards(): jnp.dot(hidden, down_experts[0], preferred_element_type=jnp.float32)  10.6 us
    ppermute x3, waiting for transfers between devices, swap(): return lax.ppermute(value, 'tp', [(0, 1), (1, 0)])  9.82 us
    ppermute x4, waiting for transfers between devices, shift(): lax.ppermute(packed, 'sp', [(i, i + distance) for i in range(count - dist...  6.41 us
  transfers between devices with their start and end apart: 8, of which 7 were waited for; matrix products, arithmetic and copies ran while one was open for 3% of the time, Pallas kernels for 0%

profile of v2, /device:TPU:14, one launch (start us, length us, event | category | flops | bytes accessed | tf_op | source)
XLA Modules:
  0.0 205.6 jit_solution(7099621895362893546)
XLA Ops:
  0.0 1.4 reduce-window.14
  1.4 0.2 slice_reduce_fusion.1
  1.6 0.1 fusion.79
  1.7 0.5 copy-done.3
  2.2 0.2 slice_reduce_fusion.2
  2.4 0.1 exponential_multiply_fusion
  2.5 1.1 copy.48
  3.6 0.8 convert.3
  4.4 1.1 copy.49
  5.5 0.8 convert.4
  6.3 1.1 copy.50
  7.4 0.2 multiply_cosine_fusion
  7.6 1.3 multiply_subtract_fusion.1
  9.0 0.3 convolution_bitcast_fusion.1
  9.3 0.2 copy.51
  9.5 0.1 reshape.231
  9.6 0.7 broadcast_in_dim.59
  10.3 0.1 broadcast_in_dim_reshape.2
  10.4 3.4 %collective-permute-start = (bf16[66,512]{1,0:T(8,128)(2,1)S(1)}, bf16[66,512]{1,0:T(8,128)(2,1)S(1)}, u32[]{:S(2)}, u32[]{:S(2)}) collective-permute-start(bf16[66,512]{1,0:T(8,128)(2,1)S(1)} %pad_maximum_fusion.9), channel_id=1, source_target_pairs={{0,2},{2,4},{4,6},{6,8},{8,10},{10,12},{12,14},{14,16},{16,18},{18... | collective-permute-start | bytes 202760 | tf_op jit(solution)/shard_map/ppermute | solution.py:21
  13.8 0.7 add_bitcast_fusion.2
  14.6 1.0 fusion.39
  15.7 2.9 %fusion.19 = f32[256,8,64]{0,2,1:T(8,128)} fusion(bf16[256,8,64]{0,2,1:T(8,128)(2,1)} %bitcast.86, f32[8,256,256]{2,1,0:T(8,128)S(1)} %fusion.39, f32[8,256]{1,0:T(8,128)S(1)} %add_bitcast_fusion.2, pred[256,256]{1,0:T(8,128)(4,1)S(1)} %iota_compare_fusion.4), kind=kOutput, calls=%fused_computation.26 | convolution fusion | flops 203423744 | bytes 2957312 | tf_op jit(solution)/shard_map/hts,she->the/dot_general | solution.py:105
  18.6 0.1 broadcast_in_dim.60
  18.7 0.1 exp.47
  18.8 0.1 copy.54
  18.9 0.1 eq.85
  19.2 3.4 %collective-permute-start.1 = (bf16[66,512]{1,0:T(8,128)(2,1)S(1)}, bf16[66,512]{1,0:T(8,128)(2,1)S(1)}, u32[]{:S(2)}, u32[]{:S(2)}) collective-permute-start(bf16[66,512]{1,0:T(8,128)(2,1)S(1)} %pad_maximum_fusion.10), channel_id=1, source_target_pairs={{0,4},{2,6},{4,8},{6,10},{8,12},{10,14},{12,16},{14,18},{16,20},{1... | collective-permute-start | bytes 202760 | tf_op jit(solution)/shard_map/ppermute | solution.py:21
  22.6 0.1 eq.81
  22.7 0.1 mul.283
  22.8 0.6 reduce-window.16
  23.4 2.0 collective-permute-done.1
  25.5 3.5 %collective-permute-start.2 = (bf16[66,512]{1,0:T(8,128)(2,1)S(1)}, bf16[66,512]{1,0:T(8,128)(2,1)S(1)}, u32[]{:S(2)}, u32[]{:S(2)}) collective-permute-start(bf16[66,512]{1,0:T(8,128)(2,1)S(1)} %pad_maximum_fusion.11), channel_id=1, source_target_pairs={{0,8},{2,10},{4,12},{6,14},{8,16},{10,18},{12,20},{14,22},{16,24},... | collective-permute-start | bytes 202760 | tf_op jit(solution)/shard_map/ppermute | solution.py:21
  29.0 0.2 slice_reduce_fusion
  29.2 2.5 %collective-permute-done.2 = bf16[66,512]{1,0:T(8,128)(2,1)S(1)} collective-permute-done((bf16[66,512]{1,0:T(8,128)(2,1)S(1)}, bf16[66,512]{1,0:T(8,128)(2,1)S(1)}, u32[]{:S(2)}, u32[]{:S(2)}) %collective-permute-start.2) | collective-permute-done | bytes 67616 | tf_op jit(solution)/shard_map/ppermute | solution.py:21
  31.9 3.0 %collective-permute-start.3 = (bf16[66,512]{1,0:T(8,128)(2,1)S(1)}, bf16[66,512]{1,0:T(8,128)(2,1)S(1)}, u32[]{:S(2)}, u32[]{:S(2)}) collective-permute-start(bf16[66,512]{1,0:T(8,128)(2,1)S(1)} %pad_maximum_fusion.12), channel_id=1, source_target_pairs={{0,16},{2,18},{4,20},{6,22},{8,24},{10,26},{12,28},{14,30},{1,17},... | collective-permute-start | bytes 202760 | tf_op jit(solution)/shard_map/ppermute | solution.py:21
  34.8 0.1 fusion.64
  34.9 1.9 collective-permute-done.3
  36.8 0.1 add_add_fusion
  36.9 0.1 copy.58
  37.0 1.4 multiply_reduce_fusion
  38.5 0.1 multiply_multiply_fusion
  38.6 0.2 copy.53
  38.8 1.1 fusion.41
  39.9 0.5 convolution_convert_fusion.1
  40.4 0.1 collective-permute-start.4
  40.5 0.1 sub.75
  40.6 0.1 copy.57
  40.7 1.7 collective-permute-done.4
  42.4 1.7 fusion.23
  44.1 0.8 convolution_convert_fusion
  44.9 56.8 %all_to_all.10 = bf16[16,32,2048]{2,1,0:T(8,128)(2,1)S(1)} all-to-all(bf16[16,32,2048]{2,1,0:T(8,128)(2,1)S(1)} %bitcast.77), channel_id=1, replica_groups=mesh['sp'=16,'tp'=2] {'sp'}, dimensions={0} | all-to-all | bytes 4194304 | tf_op jit(solution)/shard_map/all_to_all | solution.py:155
  101.7 4.2 %collective-permute-done.5 = bf16[512,2048]{1,0:T(8,128)(2,1)S(1)} collective-permute-done((bf16[512,2048]{1,0:T(8,128)(2,1)S(1)}, bf16[512,2048]{1,0:T(8,128)(2,1)S(1)}, u32[]{:S(2)}, u32[]{:S(2)}) %collective-permute-start.5) | collective-permute-done | bytes 2097184 | tf_op jit(solution)/shard_map/ppermute | solution.py:8
  105.8 11.0 %fusion.4 = f32[1024,1792]{1,0:T(8,128)S(1)} fusion(bf16[1,2048,1792]{2,1,0:T(8,128)(2,1)} %param.25, bf16[512,2048]{1,0:T(8,128)(2,1)S(1)} %bitcast.79, bf16[512,2048]{1,0:T(8,128)(2,1)S(1)} %collective-permute-done.5), kind=kOutput, calls=%fused_computation.4 | convolution fusion | flops 7524581376 | bytes 18874368 | tf_op jit(solution)/shard_map/dot_general | solution.py:53
  116.8 0.0 slice-start.3
  116.8 11.4 %fusion.2 = f32[1024,1792]{1,0:T(8,128)} fusion(bf16[1,2048,1792]{2,1,0:T(8,128)(2,1)S(1)} %bitcast.94, bf16[512,2048]{1,0:T(8,128)(2,1)S(1)} %bitcast.80, bf16[512,2048]{1,0:T(8,128)(2,1)S(1)} %collective-permute-done.5), kind=kOutput, calls=%fused_computation.2 | convolution fusion | flops 7524581376 | bytes 18874368 | tf_op jit(solution)/shard_map/dot_general | solution.py:54
  128.3 10.6 %fusion.6 = bf16[1024,2048]{1,0:T(8,128)(2,1)S(1)} fusion(bf16[1,1792,2048]{2,1,0:T(8,128)(2,1)S(1)} %bitcast.96, f32[1024,1792]{1,0:T(8,128)} %fusion.2, f32[1024,1792]{1,0:T(8,128)S(1)} %fusion.4), kind=kOutput, calls=%fused_computation.9 | convolution fusion | flops 7529299968 | bytes 26214400 | tf_op jit(solution)/shard_map/dot_general | solution.py:160
  138.9 0.2 slice.122
  139.1 0.2 collective-permute-start.6
  139.3 4.0 %collective-permute-done.6 = bf16[512,2048]{1,0:T(8,128)(2,1)S(1)} collective-permute-done((bf16[512,2048]{1,0:T(8,128)(2,1)S(1)}, bf16[512,2048]{1,0:T(8,128)(2,1)S(1)}, u32[]{:S(2)}, u32[]{:S(2)}) %collective-permute-start.6) | collective-permute-done | bytes 2097184 | tf_op jit(solution)/shard_map/ppermute | solution.py:8
  143.4 2.1 %add_convert_fusion = bf16[512,2048]{1,0:T(8,128)(2,1)} fusion(bf16[512,2048]{1,0:T(8,128)(2,1)S(1)} %collective-permute-done.6, bf16[1024,2048]{1,0:T(8,128)(2,1)S(1)} %fusion.6), kind=kLoop, calls=%fused_computation.8 | loop fusion | flops 4194304 | bytes 6291456 | tf_op jit(solution)/shard_map/convert_element_type | solution.py:167
  145.5 6.4 %all-to-all-start.1 = ((bf16[16,32,2048]{2,1,0:T(8,128)(2,1)}), bf16[16,32,2048]{2,1,0:T(8,128)(2,1)}, u32[]{:S(2)}, u32[]{:S(2)}) async-start(bf16[16,32,2048]{2,1,0:T(8,128)(2,1)} %bitcast.76), calls=%async_computation.1 | async-start | bytes 4194304 | tf_op jit(solution)/shard_map/all_to_all | solution.py:168
  151.9 48.7 %all-to-all-done.1 = bf16[16,32,2048]{2,1,0:T(8,128)(2,1)} async-done(((bf16[16,32,2048]{2,1,0:T(8,128)(2,1)}), bf16[16,32,2048]{2,1,0:T(8,128)(2,1)}, u32[]{:S(2)}, u32[]{:S(2)}) %all-to-all-start.1) | async-done | bytes 2097184 | tf_op jit(solution)/shard_map/all_to_all | solution.py:168
  200.6 2.1 %fusion.48 = f32[128,2048]{1,0:T(8,128)S(1)} fusion(bf16[512,2048]{1,0:T(8,128)(2,1)} %bitcast.32, f32[128]{0:T(128)S(1)} %get-tuple-element.36, s32[128]{0:T(128)S(1)} %get-tuple-element.38, f32[128]{0:T(128)S(1)} %get-tuple-element.35, s32[128]{0:T(128)S(1)} %get-tuple-element.37), kind=kOutput, calls=%fused_computation.71 | convolution fusion | flops 269025280 | bytes 3147776 | tf_op jit(solution)/shard_map/dot_general | solution.py:173
  202.7 2.9 %fusion.11 = bf16[128,2048]{1,0:T(8,128)(2,1)} fusion(f32[128,2048]{1,0:T(8,128)S(1)} %fusion.48, bf16[512,2048]{1,0:T(8,128)(2,1)} %bitcast.32, bf16[128,2048]{1,0:T(8,128)(2,1)S(1)} %get-tuple-element.42, f32[128]{0:T(128)S(1)} %get-tuple-element.36, s32[128]{0:T(128)S(1)} %get-tuple-element.38, f32[128]{0:T(128)S(1)} %get-tuple-element.35, ...), kind=kOutput, calls=%fused_computation.14 | convolution fusion | flops 269877248 | bytes 4196352 | tf_op jit(solution)/shard_map/dot_general | solution.py:173
  (63 shorter events, 0.5 us)
Async XLA Ops:
  0.0 39.9 %copy-start = (bf16[512,2048]{1,0:T(8,128)(2,1)S(1)}, bf16[512,2048]{1,0:T(8,128)(2,1)}, u32[]{:S(2)}) copy-start(bf16[512,2048]{1,0:T(8,128)(2,1)} %param.20) | copy-start | bytes 6291460
  1.6 0.6 copy-start.3
  2.4 6.9 %copy-start.5 = (f32[8]{0:T(128)}, f32[8]{0:T(128)S(1)}, u32[]{:S(2)}) copy-start(f32[8]{0:T(128)S(1)} %slice_reduce_fusion.2) | copy-start | bytes 100
  7.4 1.6 copy-start.2
  9.6 9.0 %copy-start.6 = (f32[8]{0:T(128)S(1)}, f32[8]{0:T(128)}, u32[]{:S(2)}) copy-start(f32[8]{0:T(128)} %copy-done.5) | copy-start | bytes 100
  9.6 9.2 %copy-start.7 = (s32[128,2]{0,1:T(2,128)S(1)}, s32[128,2]{0,1:T(2,128)}, u32[]{:S(2)}) copy-start(s32[128,2]{0,1:T(2,128)} %param.23) | copy-start | bytes 3076
  10.4 8.6 %collective-permute-start = (bf16[66,512]{1,0:T(8,128)(2,1)S(1)}, bf16[66,512]{1,0:T(8,128)(2,1)S(1)}, u32[]{:S(2)}, u32[]{:S(2)}) collective-permute-start(bf16[66,512]{1,0:T(8,128)(2,1)S(1)} %pad_maximum_fusion.9), channel_id=1, source_target_pairs={{0,2},{2,4},{4,6},{6,8},{8,10},{10,12},{12,14},{14,16},{16,18},{18... | collective-permute-start | bytes 202760 | tf_op jit(solution)/shard_map/ppermute | solution.py:21
  14.6 8.1 %copy-start.8 = (f32[512]{0:T(512)S(1)}, f32[512]{0:T(512)}, u32[]{:S(2)}) copy-start(f32[512]{0:T(512)} %param.19) | copy-start | bytes 6148
  19.2 6.2 %collective-permute-start.1 = (bf16[66,512]{1,0:T(8,128)(2,1)S(1)}, bf16[66,512]{1,0:T(8,128)(2,1)S(1)}, u32[]{:S(2)}, u32[]{:S(2)}) collective-permute-start(bf16[66,512]{1,0:T(8,128)(2,1)S(1)} %pad_maximum_fusion.10), channel_id=1, source_target_pairs={{0,4},{2,6},{4,8},{6,10},{8,12},{10,14},{12,16},{14,18},{16,20},{1... | collective-permute-start | bytes 202760 | tf_op jit(solution)/shard_map/ppermute | solution.py:21
  25.5 6.2 %collective-permute-start.2 = (bf16[66,512]{1,0:T(8,128)(2,1)S(1)}, bf16[66,512]{1,0:T(8,128)(2,1)S(1)}, u32[]{:S(2)}, u32[]{:S(2)}) collective-permute-start(bf16[66,512]{1,0:T(8,128)(2,1)S(1)} %pad_maximum_fusion.11), channel_id=1, source_target_pairs={{0,8},{2,10},{4,12},{6,14},{8,16},{10,18},{12,20},{14,22},{16,24},... | collective-permute-start | bytes 202760 | tf_op jit(solution)/shard_map/ppermute | solution.py:21
  31.9 5.0 %collective-permute-start.3 = (bf16[66,512]{1,0:T(8,128)(2,1)S(1)}, bf16[66,512]{1,0:T(8,128)(2,1)S(1)}, u32[]{:S(2)}, u32[]{:S(2)}) collective-permute-start(bf16[66,512]{1,0:T(8,128)(2,1)S(1)} %pad_maximum_fusion.12), channel_id=1, source_target_pairs={{0,16},{2,18},{4,20},{6,22},{8,24},{10,26},{12,28},{14,30},{1,17},... | collective-permute-start | bytes 202760 | tf_op jit(solution)/shard_map/ppermute | solution.py:21
  38.6 5.5 %copy-start.4 = (f32[2048]{0:T(1024)S(1)}, f32[2048]{0:T(1024)}, u32[]{:S(2)}) copy-start(f32[2048]{0:T(1024)} %param.22) | copy-start | bytes 24580
  40.4 2.0 collective-permute-start.4
  101.7 15.1 %slice-start = ((s8[7340032]{0:T(1024)(128)(4,1)}), s8[4194304]{0:T(1024)(128)(4,1)S(1)}, s32[]{:S(2)}) async-start(s8[7340032]{0:T(1024)(128)(4,1)} %bitcast.93), calls=%async_computation.2 | async-start | bytes 8388608
  101.7 15.1 %slice-start.1 = ((s8[7340032]{0:T(1024)(128)(4,1)}), s8[3145728]{0:T(1024)(128)(4,1)S(1)}, s32[]{:S(2)}) async-start(s8[7340032]{0:T(1024)(128)(4,1)} %bitcast.93), calls=%async_computation.3 | async-start | bytes 6291456
  101.7 4.2 %collective-permute-start.5 = (bf16[512,2048]{1,0:T(8,128)(2,1)S(1)}, bf16[512,2048]{1,0:T(8,128)(2,1)S(1)}, u32[]{:S(2)}, u32[]{:S(2)}) collective-permute-start(bf16[512,2048]{1,0:T(8,128)(2,1)S(1)} %bitcast.78), channel_id=1, source_target_pairs={{0,1},{1,0},{2,3},{3,2},{4,5},{5,4},{6,7},{7,6},{8,9},{9,8},{10,11... | collective-permute-start | bytes 6291464 | tf_op jit(solution)/shard_map/ppermute | solution.py:8
  105.8 22.5 %slice-start.2 = ((s8[7340032]{0:T(1024)(128)(4,1)}), s8[4194304]{0:T(1024)(128)(4,1)S(1)}, s32[]{:S(2)}) async-start(s8[7340032]{0:T(1024)(128)(4,1)} %bitcast.95), calls=%async_computation.4 | async-start | bytes 8388608
  116.8 11.5 %slice-start.3 = ((s8[7340032]{0:T(1024)(128)(4,1)}), s8[3145728]{0:T(1024)(128)(4,1)S(1)}, s32[]{:S(2)}) async-start(s8[7340032]{0:T(1024)(128)(4,1)} %bitcast.95), calls=%async_computation.5 | async-start | bytes 6291456
  139.1 12.7 %copy-start.9 = (f32[128,2]{0,1:T(2,128)S(1)}, f32[128,2]{0,1:T(2,128)}, u32[]{:S(2)}) copy-start(f32[128,2]{0,1:T(2,128)} %param.24) | copy-start | bytes 3076
  139.1 4.2 %collective-permute-start.6 = (bf16[512,2048]{1,0:T(8,128)(2,1)S(1)}, bf16[512,2048]{1,0:T(8,128)(2,1)S(1)}, u32[]{:S(2)}, u32[]{:S(2)}) collective-permute-start(bf16[512,2048]{1,0:T(8,128)(2,1)S(1)} %slice.122), channel_id=1, source_target_pairs={{0,1},{1,0},{2,3},{3,2},{4,5},{5,4},{6,7},{7,6},{8,9},{9,8},{10,11... | collective-permute-start | bytes 6291464 | tf_op jit(solution)/shard_map/ppermute | solution.py:8
  145.5 55.1 %all-to-all-start.1 = ((bf16[16,32,2048]{2,1,0:T(8,128)(2,1)}), bf16[16,32,2048]{2,1,0:T(8,128)(2,1)}, u32[]{:S(2)}, u32[]{:S(2)}) async-start(bf16[16,32,2048]{2,1,0:T(8,128)(2,1)} %bitcast.76), calls=%async_computation.1 | async-start | bytes 4194304 | tf_op jit(solution)/shard_map/all_to_all | solution.py:168
  151.8 53.8 %copy-start.1 = (bf16[512,2048]{1,0:T(8,128)(2,1)S(1)}, bf16[512,2048]{1,0:T(8,128)(2,1)}, u32[]{:S(2)}) copy-start(bf16[512,2048]{1,0:T(8,128)(2,1)} %param.20) | copy-start | bytes 6291460
